TPU v7x, 256 devices: a 4x2x16 block of a 4x16x16 slice. The times are simulated.
256 devices in a mesh: grp: 2 (over y), sp: 16 (over z), tp: 8 (over x, core).
Axes of the slice: x: 4, y: 2, z: 16, core: 2. Of those that a mesh axis runs over, the one named last changes fastest.
The devices are a block of a 4x16x16 slice.
Arguments:
- layer_input: bfloat16 [64, 6144, 2048], P(('grp', 'tp'), 'sp'), parts along dimension 0, may hold values from -6 to 6
- input_gain: float32 [2048], replicated, may hold values from 0.1 to 1.9
- key_weight: bfloat16 [2048, 512], replicated, may hold values from -0.125 to 0.125
- value_weight: bfloat16 [2048, 512], replicated, may hold values from -0.125 to 0.125
- stick_offsets: bfloat16 [4, 64, 6144], P(None, ('grp', 'tp'), 'sp'), parts along dimension 1
- head_bias: float32 [16], replicated
- queries: bfloat16 [16, 16, 512], P(('grp', 'tp'), 'sp'), parts along dimension 0, may hold values from -6 to 6
Outputs:
- key_cache: bfloat16 [16, 16, 6144, 128], P(('grp', 'tp'), 'sp'), parts along dimension 0
- value_cache: bfloat16 [16, 16, 6144, 128], P(('grp', 'tp'), 'sp'), parts along dimension 0
- offset_cache: bfloat16 [16, 16, 6144], P(('grp', 'tp'), 'sp'), parts along dimension 0
- first_read: bfloat16 [16, 16, 512], P(('grp', 'tp'), 'sp'), parts along dimension 0
There are 2 independent parts, one for each index of `grp`. A program takes and returns all parts, laid end to end along the dimension named above; an argument that names none is the same for every part. Nothing has to cross between parts.
All inputs are finite; a program needn't handle non-finite values.
Results may differ from a plain program's by a relative error of at most 0.014.
Values may be sent and summed in bfloat16 or wider, within the bound.
A program may use at most 64 MiB of HBM per device.

v0:
```python
import math

import jax
import jax.numpy as jnp
from jax import lax
from jax.sharding import PartitionSpec as P

H = 16
KVH = 4
HD = 128


EPSILON = 1e-06


def rms_scale(matrix):
    return matrix * lax.rsqrt(jnp.mean(matrix * matrix, axis=-1, keepdims=True) + EPSILON)


def stick_weights(scores, spread, carried):
    inside = lax.cumsum(spread, axis=scores.ndim - 1, reverse=True) - spread
    return jnp.exp(jax.nn.log_sigmoid(scores) - inside - carried)


def normalize(rows, input_gain):
    return (rms_scale(rows.astype(jnp.float32)) * input_gain).astype(jnp.bfloat16)


def project(normed_rows, weight):
    return jnp.dot(normed_rows, weight, preferred_element_type=jnp.float32).astype(jnp.bfloat16)


def shards(layer_input, input_gain, key_weight, value_weight, stick_offsets, head_bias, queries):
    seq_count, block_len, model_width = layer_input.shape
    sp_count = lax.axis_size("sp")
    group_size = H // KVH
    length = sp_count * block_len
    offset_lookup_matrix = head_bias.reshape(KVH, group_size)
    offset_parts = jnp.transpose(stick_offsets, (1, 0, 2)).reshape(sp_count, block_len)
    head_index = lax.axis_index("sp") % KVH
    normed_rows = normalize(layer_input.reshape(seq_count * block_len, model_width), input_gain)
    key_rows = project(normed_rows, key_weight).reshape(seq_count, block_len, KVH, HD)
    value_rows = project(normed_rows, value_weight).reshape(seq_count, block_len, KVH, HD)
    key_rows, value_rows = (key_rows, value_rows)
    key_parts = jnp.transpose(key_rows, (0, 2, 1, 3)).reshape(sp_count, block_len, HD)
    value_parts = jnp.transpose(value_rows, (0, 2, 1, 3)).reshape(sp_count, block_len, HD)
    key_cache, value_cache, offset_cache = (
        lax.all_to_all(key_parts, "sp", split_axis=0, concat_axis=1, tiled=True),
        lax.all_to_all(value_parts, "sp", split_axis=0, concat_axis=1, tiled=True),
        lax.all_to_all(offset_parts, "sp", split_axis=0, concat_axis=1, tiled=True),
    )
    key_cache = key_cache.reshape(1, 1, length, HD)
    value_cache = value_cache.reshape(1, 1, length, HD)
    offset_cache = offset_cache.reshape(1, 1, length)
    bias_row = lax.dynamic_index_in_dim(offset_lookup_matrix, head_index, 0, keepdims=False)
    own_query = queries.reshape(group_size, HD)
    scores = lax.dot_general(
        own_query,
        key_cache.reshape(length, HD),
        (((1,), (1,)), ((), ())),
        preferred_element_type=jnp.float32,
    )
    scores = (
        scores / math.sqrt(HD)
        + bias_row[:, None]
        + offset_cache.reshape(1, length).astype(jnp.float32)
    )
    spread = jax.nn.softplus(scores)
    weights = stick_weights(scores, spread, 0.0).astype(jnp.bfloat16)
    mixture = jnp.dot(weights, value_cache.reshape(length, HD), preferred_element_type=jnp.float32)
    first_read = rms_scale(mixture).astype(jnp.bfloat16).reshape(1, 1, group_size * HD)
    return (key_cache, value_cache, offset_cache, first_read)


def solution(mesh):
    placed = (
        P(("grp", "tp"), "sp", None),
        P(),
        P(),
        P(),
        P(None, ("grp", "tp"), "sp"),
        P(),
        P(("grp", "tp"), "sp", None),
    )
    return jax.shard_map(
        shards,
        mesh=mesh,
        in_specs=placed,
        out_specs=(
            P(("grp", "tp"), "sp", None, None),
            P(("grp", "tp"), "sp", None, None),
            P(("grp", "tp"), "sp", None),
            P(("grp", "tp"), "sp", None),
        ),
        check_vma=False,
    )
```

profile of v0, /device:TPU:36, one launch (start us, length us, event | category | flops | bytes accessed | tf_op | source)
XLA Modules:
  0.0 223.7 jit_solution(14037182767658850946)
XLA Ops:
  0.6 0.9 copy.16
  1.5 0.5 broadcast.51
  2.0 0.7 reduce.4
  2.8 0.7 reshape.127
  3.4 24.0 %all-to-all-start.2 = ((bf16[16,2,192]{2,1,0:T(2,128)(2,1)}), bf16[16,2,192]{2,1,0:T(2,128)(2,1)S(1)}, u32[]{:S(2)}, u32[]{:S(2)}) async-start(bf16[16,2,192]{2,1,0:T(2,128)(2,1)} %reshape.127), calls=%async_computation.2 | async-start | bytes 32768 | tf_op jit(solution)/shard_map/all_to_all | solution.py:50
  27.4 4.1 %multiply_reduce_fusion = f32[4,384]{1,0:T(4,128)S(1)} fusion(bf16[4,384,2048]{2,1,0:T(8,128)(2,1)} %param.7), kind=kLoop, calls=%fused_computation.3 | loop fusion | flops 9435648 | bytes 6297600 | tf_op jit(solution)/shard_map/reduce_sum | solution.py:17
  31.6 4.3 %fusion.1 = bf16[1536,2048]{1,0:T(8,128)(2,1)S(1)} fusion(f32[2048]{0:T(1024)S(1)} %copy-done.3, f32[1536]{0:T(1024)S(1)} %rsqrt.20, bf16[4,384,2048]{2,1,0:T(8,128)(2,1)} %param.7), kind=kLoop, calls=%fused_computation.2 | loop fusion | flops 12582912 | bytes 12597248 | tf_op jit(solution)/shard_map/convert_element_type | solution.py:26
  35.9 2.7 %copy-done.1 = bf16[1536,2048]{1,0:T(8,128)(2,1)} copy-done((bf16[1536,2048]{1,0:T(8,128)(2,1)}, bf16[1536,2048]{1,0:T(8,128)(2,1)S(1)}, u32[]{:S(2)}) %copy-start.1) | copy-done | bytes 6291480
  38.5 4.5 %convolution_convert_fusion.1 = bf16[1536,512]{1,0:T(8,128)(2,1)} fusion(bf16[1536,2048]{1,0:T(8,128)(2,1)S(1)} %fusion.1, bf16[2048,512]{1,0:T(8,128)(2,1)S(1)} %copy-done), kind=kOutput, calls=%fused_computation.9 | convolution fusion | flops 3222011904 | bytes 9961472 | tf_op jit(solution)/shard_map/dot_general | solution.py:30
  43.0 3.5 %reshape.111 = bf16[4,384,4,128]{3,2,1,0:T(4,128)(2,1)} reshape(bf16[1536,512]{1,0:T(8,128)(2,1)} %convolution_convert_fusion.1) | data formatting | bytes 3145728 | tf_op jit(solution)/shard_map/reshape | solution.py:42
  46.5 2.9 %copy.14 = bf16[4,384,4,128]{3,1,2,0:T(8,128)(2,1)} copy(bf16[4,384,4,128]{3,2,1,0:T(4,128)(2,1)} %reshape.111) | data formatting | bytes 3145728 | tf_op jit(solution)/shard_map/reshape | solution.py:42
  49.4 12.0 %all-to-all-start = ((bf16[16,384,128]{2,1,0:T(8,128)(2,1)}), bf16[16,384,128]{2,1,0:T(8,128)(2,1)}, u32[]{:S(2)}, u32[]{:S(2)}) async-start(bf16[16,384,128]{2,1,0:T(8,128)(2,1)} %bitcast.47), calls=%async_computation | async-start | bytes 3145728 | tf_op jit(solution)/shard_map/all_to_all | solution.py:48
  61.4 8.0 %convolution_convert_fusion = bf16[1536,512]{1,0:T(8,128)(2,1)} fusion(bf16[1536,2048]{1,0:T(8,128)(2,1)} %copy-done.1, bf16[2048,512]{1,0:T(8,128)(2,1)} %param.10), kind=kOutput, calls=%fused_computation.8 | convolution fusion | flops 3222011904 | bytes 9961472 | tf_op jit(solution)/shard_map/dot_general | solution.py:30
  69.4 3.5 %reshape.114 = bf16[4,384,4,128]{3,2,1,0:T(4,128)(2,1)} reshape(bf16[1536,512]{1,0:T(8,128)(2,1)} %convolution_convert_fusion) | data formatting | bytes 3145728 | tf_op jit(solution)/shard_map/reshape | solution.py:43
  72.9 2.9 %copy.15 = bf16[4,384,4,128]{3,1,2,0:T(8,128)(2,1)} copy(bf16[4,384,4,128]{3,2,1,0:T(4,128)(2,1)} %reshape.114) | data formatting | bytes 3145728 | tf_op jit(solution)/shard_map/reshape | solution.py:43
  75.8 59.2 %all-to-all-done = bf16[16,384,128]{2,1,0:T(8,128)(2,1)} async-done(((bf16[16,384,128]{2,1,0:T(8,128)(2,1)}), bf16[16,384,128]{2,1,0:T(8,128)(2,1)}, u32[]{:S(2)}, u32[]{:S(2)}) %all-to-all-start) | async-done | bytes 1572896 | tf_op jit(solution)/shard_map/all_to_all | solution.py:48
  135.0 6.4 %all-to-all-start.1 = ((bf16[16,384,128]{2,1,0:T(8,128)(2,1)}), bf16[16,384,128]{2,1,0:T(8,128)(2,1)}, u32[]{:S(2)}, u32[]{:S(2)}) async-start(bf16[16,384,128]{2,1,0:T(8,128)(2,1)} %bitcast.46), calls=%async_computation.1 | async-start | bytes 3145728 | tf_op jit(solution)/shard_map/all_to_all | solution.py:49
  141.7 1.9 fusion.4
  143.7 5.0 %reduce-window.6 = f32[4,48,128]{2,1,0:T(8,128)S(1)} reduce-window(f32[4,48,128]{2,1,0:T(8,128)S(1)} %bitcast.48, f32[]{:T(128)} %constant.33.clone.1), window={size=1x1x128 pad=0_0x0_0x0_127}, to_apply=%region_1.2 | reduce-window | flops 3121152 | bytes 196612 | tf_op jit(solution)/shard_map/reduce-window
  149.4 66.3 %all-to-all-done.1 = bf16[16,384,128]{2,1,0:T(8,128)(2,1)} async-done(((bf16[16,384,128]{2,1,0:T(8,128)(2,1)}), bf16[16,384,128]{2,1,0:T(8,128)(2,1)}, u32[]{:S(2)}, u32[]{:S(2)}) %all-to-all-start.1) | async-done | bytes 1572896 | tf_op jit(solution)/shard_map/all_to_all | solution.py:49
  215.7 2.0 multiply_reduce_fusion.1
  217.8 0.6 reshape.122
  218.4 2.7 %copy.28 = bf16[1,1,6144,128]{3,2,1,0:T(8,128)(2,1)} copy(bf16[1,1,6144,128]{3,2,1,0:T(8,128)(2,1)} %bitcast.3) | data formatting | bytes 3145728
  221.0 2.7 %copy.29 = bf16[1,1,6144,128]{3,2,1,0:T(8,128)(2,1)} copy(bf16[1,1,6144,128]{3,2,1,0:T(8,128)(2,1)} %bitcast.6) | data formatting | bytes 3145728
  (28 shorter events, 1.1 us)
Async XLA Ops:
  0.6 37.9 %copy-start = (bf16[2048,512]{1,0:T(8,128)(2,1)S(1)}, bf16[2048,512]{1,0:T(8,128)(2,1)}, u32[]{:S(2)}) copy-start(bf16[2048,512]{1,0:T(8,128)(2,1)} %param.9) | copy-start | bytes 6291460
  3.4 45.9 %all-to-all-start.2 = ((bf16[16,2,192]{2,1,0:T(2,128)(2,1)}), bf16[16,2,192]{2,1,0:T(2,128)(2,1)S(1)}, u32[]{:S(2)}, u32[]{:S(2)}) async-start(bf16[16,2,192]{2,1,0:T(2,128)(2,1)} %reshape.127), calls=%async_computation.2 | async-start | bytes 32768 | tf_op jit(solution)/shard_map/all_to_all | solution.py:50
  27.4 4.1 %copy-start.3 = (f32[2048]{0:T(1024)S(1)}, f32[2048]{0:T(1024)}, u32[]{:S(2)}) copy-start(f32[2048]{0:T(1024)} %param.8) | copy-start | bytes 24580
  35.8 2.7 %copy-start.1 = (bf16[1536,2048]{1,0:T(8,128)(2,1)}, bf16[1536,2048]{1,0:T(8,128)(2,1)S(1)}, u32[]{:S(2)}) copy-start(bf16[1536,2048]{1,0:T(8,128)(2,1)S(1)} %fusion.1) | copy-start | bytes 18874372
  49.4 85.6 %all-to-all-start = ((bf16[16,384,128]{2,1,0:T(8,128)(2,1)}), bf16[16,384,128]{2,1,0:T(8,128)(2,1)}, u32[]{:S(2)}, u32[]{:S(2)}) async-start(bf16[16,384,128]{2,1,0:T(8,128)(2,1)} %bitcast.47), calls=%async_computation | async-start | bytes 3145728 | tf_op jit(solution)/shard_map/all_to_all | solution.py:48
  75.8 65.6 %copy-start.4 = (bf16[1,1,512]{2,1,0:T(2,128)(2,1)S(1)}, bf16[1,1,512]{2,1,0:T(2,128)(2,1)}, u32[]{:S(2)}) copy-start(bf16[1,1,512]{2,1,0:T(2,128)(2,1)} %param.13) | copy-start | bytes 3076
  75.8 65.6 %copy-start.5 = (f32[16]{0:T(128)S(1)}, f32[16]{0:T(128)}, u32[]{:S(2)}) copy-start(f32[16]{0:T(128)} %param.12) | copy-start | bytes 196
  135.0 80.8 %all-to-all-start.1 = ((bf16[16,384,128]{2,1,0:T(8,128)(2,1)}), bf16[16,384,128]{2,1,0:T(8,128)(2,1)}, u32[]{:S(2)}, u32[]{:S(2)}) async-start(bf16[16,384,128]{2,1,0:T(8,128)(2,1)} %bitcast.46), calls=%async_computation.1 | async-start | bytes 3145728 | tf_op jit(solution)/shard_map/all_to_all | solution.py:49
  141.6 76.1 %copy-start.2 = (bf16[16,1,384]{2,1,0:T(2,128)(2,1)}, bf16[16,1,384]{2,1,0:T(2,128)(2,1)S(1)}, u32[]{:S(2)}) copy-start(bf16[16,1,384]{2,1,0:T(2,128)(2,1)S(1)} %reshape.128) | copy-start | bytes 36868
where the time goes:
time: 224 us
  waiting for transfers between devices  126 us (56%)
  starting transfers between devices  42.4 us (19%)
  local copies, waits for them, and re-layouts  23.8 us (11%)
  matrix products  16.4 us (7%)
  other arithmetic  14.8 us (7%)
    all_to_all x1, waiting for transfers between devices, shards(): lax.all_to_all(value_parts, 'sp', split_axis=0, concat_axis=1, tiled=True)  66.3 us
    all_to_all x1, waiting for transfers between devices, shards(): lax.all_to_all(key_parts, 'sp', split_axis=0, concat_axis=1, tiled=True)  59.2 us
    all_to_all x1, starting transfers between devices, shards(): lax.all_to_all(offset_parts, 'sp', split_axis=0, concat_axis=1, tiled=True)  24 us
    dot_general x2, matrix products, project(): jnp.dot(normed_rows, weight, preferred_element_type=jnp.float32)  12.5 us
    all_to_all x1, starting transfers between devices, shards(): lax.all_to_all(key_parts, 'sp', split_axis=0, concat_axis=1, tiled=True)  12 us
    unnamed x17, local copies, waits for them, and re-layouts  8.78 us
    all_to_all x1, starting transfers between devices, shards(): lax.all_to_all(value_parts, 'sp', split_axis=0, concat_axis=1, tiled=True)  6.41 us
    reshape x2, local copies, waits for them, and re-layouts, shards(): project(normed_rows, value_weight).reshape(seq_count, block_len, KVH, HD)  6.38 us
  transfers between devices with their start and end apart: 3, of which 2 were waited for; matrix products, arithmetic and copies ran while one was open for 19% of the time, Pallas kernels for 0%

commit v1 on v0

v1 whole, which is shorter than its diff:
```python
import functools
import math

import jax
import jax.numpy as jnp
from jax import lax
from jax.experimental import pallas as pl
from jax.experimental.pallas import tpu as pltpu
from jax.sharding import PartitionSpec as P

H = 16
KVH = 4
HD = 128
EPSILON = 1e-06
MESH = pl.DeviceIdType.MESH
NORM_ROWS = 16


def split_rows(row, count):
    return [row[:, k * HD : (k + 1) * HD] for k in range(count)]


def kernel(
    n,
    x_ref, gain_ref, wk_ref, wv_ref, off_ref, bias_ref, q_ref,
    key_ref, value_ref, off_out_ref, read_ref,
    x_buf, w_buf, normed, sent, held, off_sent, off_held, later, mixes, totals,
    x_sem, w_sem, send_sem, recv_sem, off_send_sem, off_recv_sem, out_sem, chain, ready,
):
    prompts, block, _ = x_ref.shape
    group = H // KVH
    lane_rows = block // HD
    me = lax.axis_index("sp")
    barrier = pltpu.get_barrier_semaphore()
    pl.semaphore_signal(barrier, inc=1, device_id={"sp": lax.rem(me + n - 1, n)}, device_id_type=MESH)

    def x_copy(i):
        return pltpu.make_async_copy(x_ref.at[i], x_buf.at[i], x_sem.at[i])

    def w_copies(h):
        columns = pl.ds(h * HD, HD)
        return (
            pltpu.make_async_copy(wk_ref.at[:, columns], w_buf.at[h, :, pl.ds(0, HD)], w_sem.at[h, 0]),
            pltpu.make_async_copy(wv_ref.at[:, columns], w_buf.at[h, :, pl.ds(HD, HD)], w_sem.at[h, 1]),
        )

    x_copy(0).start()
    for h in range(KVH):
        for copy in w_copies(h):
            copy.start()
    for i in range(1, prompts):
        x_copy(i).start()

    for h in range(KVH):
        rows = off_ref[h].astype(jnp.float32)
        for i in range(prompts):
            pieces = split_rows(rows[i : i + 1], lane_rows)
            off_sent[i * KVH + h] = jnp.concatenate(pieces + pieces[:1], axis=0).astype(jnp.bfloat16)
    below = lax.broadcasted_iota(jnp.int32, (block, block), 0)
    across = lax.broadcasted_iota(jnp.int32, (block, block), 1)
    later[...] = jnp.where(below > across, 1.0, 0.0).astype(jnp.bfloat16)

    pl.semaphore_wait(barrier, 1)

    @pl.when(me > 0)
    def _():
        pl.semaphore_wait(chain, 1)

    def announce(t, carry):
        pl.semaphore_signal(ready.at[me], inc=1, device_id={"sp": t}, device_id_type=MESH)
        return carry

    lax.fori_loop(0, me, announce, 0)

    @pl.when(me < n - 1)
    def _():
        pl.semaphore_signal(chain, inc=1, device_id={"sp": lax.rem(me + 1, n)}, device_id_type=MESH)

    def copies(t, slot):
        to = {"sp": t}
        return (
            pltpu.make_async_remote_copy(
                sent.at[t, 0], held.at[slot, 0], send_sem.at[t, 0], recv_sem.at[slot, 0], device_id=to, device_id_type=MESH
            ),
            pltpu.make_async_remote_copy(
                sent.at[t, 1], held.at[slot, 1], send_sem.at[t, 1], recv_sem.at[slot, 1], device_id=to, device_id_type=MESH
            ),
            pltpu.make_async_remote_copy(
                off_sent.at[t], off_held.at[slot], off_send_sem.at[t], off_recv_sem.at[slot], device_id=to, device_id_type=MESH
            ),
        )

    def send(t):
        for copy in copies(t, me):
            copy.start()

    def project_prompt(i, carry):
        x_copy(i).wait()

        def norm(r, carry):
            rows = pl.ds(pl.multiple_of(r * NORM_ROWS, NORM_ROWS), NORM_ROWS)
            x = x_buf[i, rows, :].astype(jnp.float32)
            scale = lax.rsqrt(jnp.mean(x * x, axis=-1, keepdims=True) + EPSILON)
            normed[rows, :] = (x * scale * gain_ref[...]).astype(jnp.bfloat16)
            return carry

        lax.fori_loop(0, block // NORM_ROWS, norm, 0)

        def project_head(h, carry):
            t = i * KVH + h

            @pl.when(i == 0)
            def _():
                for copy in w_copies(h):
                    copy.wait()

            rows = jnp.dot(normed[...], w_buf[h], preferred_element_type=jnp.float32).astype(jnp.bfloat16)

            @pl.when(t != me)
            def _():
                sent[t, 0] = rows[:, :HD]
                sent[t, 1] = rows[:, HD:]

            @pl.when(t == me)
            def _():
                held[me, 0] = rows[:, :HD]
                held[me, 1] = rows[:, HD:]
                off_held[me] = off_sent[t]

            @pl.when(jnp.logical_and(t >= 1, t - 1 < me))
            def _():
                send(t - 1)

            return carry

        lax.fori_loop(0, KVH, project_head, 0)
        return carry

    lax.fori_loop(0, prompts, project_prompt, 0)

    def send_later(t, carry):
        pl.semaphore_wait(ready.at[t], 1)
        send(t)
        return carry

    lax.fori_loop(me + 1, n, send_later, 0)

    head = lax.rem(me, KVH)
    row_index = lax.broadcasted_iota(jnp.int32, (2 * group, 1), 0)
    query_rows = split_rows(q_ref[0], group)
    query = jnp.concatenate(query_rows + query_rows, axis=0)
    bias = jnp.zeros((2 * group, 1), jnp.float32)
    for g in range(group):
        bias = jnp.where(lax.rem(row_index, group) == g, bias_ref[head * group + g], bias)

    def out_copies(slot):
        rows = pl.ds(pl.multiple_of(slot * block, block), block)
        return (
            pltpu.make_async_copy(held.at[slot, 0], key_ref.at[0, 0, rows, :], out_sem.at[slot, 0]),
            pltpu.make_async_copy(held.at[slot, 1], value_ref.at[0, 0, rows, :], out_sem.at[slot, 1]),
        )

    def read_block(j, carry):
        slot = lax.rem(me + j, n)

        @pl.when(j > 0)
        def _():
            for copy in copies(slot, slot):
                copy.wait_recv()

        for copy in out_copies(slot):
            copy.start()
        off_rows = off_held[slot].astype(jnp.float32)
        off_row = jnp.concatenate([off_rows[k : k + 1] for k in range(lane_rows)], axis=1)
        off_out_ref[0, :, pl.ds(pl.multiple_of(slot * block, HD), block)] = off_row.astype(jnp.bfloat16)
        scores = lax.dot_general(query, held[slot, 0], (((1,), (1,)), ((), ())), preferred_element_type=jnp.float32)
        scores = scores * (1.0 / math.sqrt(HD)) + bias + off_row
        tail = jnp.log1p(jnp.exp(-jnp.abs(scores)))
        spread = jnp.maximum(scores, 0.0) + tail
        log_take = jnp.minimum(scores, 0.0) - tail
        high = spread.astype(jnp.bfloat16)
        rest = spread - high.astype(jnp.float32)
        middle = rest.astype(jnp.bfloat16)
        low = (rest - middle.astype(jnp.float32)).astype(jnp.bfloat16)
        inside = (
            jnp.dot(high, later[...], preferred_element_type=jnp.float32)
            + jnp.dot(middle, later[...], preferred_element_type=jnp.float32)
            + jnp.dot(low, later[...], preferred_element_type=jnp.float32)
        )
        weights = jnp.exp(log_take - inside)
        coarse = weights.astype(jnp.bfloat16)
        fine = (weights - coarse.astype(jnp.float32)).astype(jnp.bfloat16)
        both = jnp.where(row_index < group, coarse.astype(jnp.float32), fine.astype(jnp.float32)).astype(jnp.bfloat16)
        mixes[slot] = jnp.dot(both, held[slot, 1], preferred_element_type=jnp.float32)
        totals[slot] = jnp.broadcast_to(jnp.sum(spread, axis=-1, keepdims=True), (2 * group, HD))
        return carry

    lax.fori_loop(0, n, read_block, 0)

    def fold(j, carry):
        mixture, beyond = carry
        slot = n - 1 - j
        return mixture + jnp.exp(-beyond) * mixes[slot], beyond + totals[slot]

    zeros = jnp.zeros((2 * group, HD), jnp.float32)
    mixture, _ = lax.fori_loop(0, n, fold, (zeros, zeros))
    mixture = mixture[:group] + mixture[group:]
    mixture = mixture * lax.rsqrt(jnp.mean(mixture * mixture, axis=-1, keepdims=True) + EPSILON)
    read_ref[0] = jnp.concatenate([mixture[g : g + 1] for g in range(group)], axis=1).astype(jnp.bfloat16)

    def finish(j, carry):
        slot = lax.rem(me + j, n)

        @pl.when(j > 0)
        def _():
            for copy in copies(slot, slot):
                copy.wait_send()

        for copy in out_copies(slot):
            copy.wait()
        return carry

    lax.fori_loop(0, n, finish, 0)


def shards(layer_input, input_gain, key_weight, value_weight, stick_offsets, head_bias, queries):
    seq_count, block, width = layer_input.shape
    n = lax.axis_size("sp")
    length = n * block
    group = H // KVH
    hbm = pl.BlockSpec(memory_space=pl.ANY)
    vmem = pl.BlockSpec(memory_space=pltpu.VMEM)
    smem = pl.BlockSpec(memory_space=pltpu.SMEM)
    return pl.pallas_call(
        functools.partial(kernel, n),
        out_shape=(
            jax.ShapeDtypeStruct((1, 1, length, HD), jnp.bfloat16),
            jax.ShapeDtypeStruct((1, 1, length, HD), jnp.bfloat16),
            jax.ShapeDtypeStruct((1, 1, length), jnp.bfloat16),
            jax.ShapeDtypeStruct((1, 1, group * HD), jnp.bfloat16),
        ),
        in_specs=[hbm, vmem, hbm, hbm, vmem, smem, vmem],
        out_specs=(hbm, hbm, vmem, vmem),
        scratch_shapes=[
            pltpu.VMEM((seq_count, block, width), jnp.bfloat16),
            pltpu.VMEM((KVH, width, 2 * HD), jnp.bfloat16),
            pltpu.VMEM((block, width), jnp.bfloat16),
            pltpu.VMEM((n, 2, block, HD), jnp.bfloat16),
            pltpu.VMEM((n, 2, block, HD), jnp.bfloat16),
            pltpu.VMEM((n, 4, HD), jnp.bfloat16),
            pltpu.VMEM((n, 4, HD), jnp.bfloat16),
            pltpu.VMEM((block, block), jnp.bfloat16),
            pltpu.VMEM((n, 2 * group, HD), jnp.float32),
            pltpu.VMEM((n, 2 * group, HD), jnp.float32),
            pltpu.SemaphoreType.DMA((seq_count,)),
            pltpu.SemaphoreType.DMA((KVH, 2)),
            pltpu.SemaphoreType.DMA((n, 2)),
            pltpu.SemaphoreType.DMA((n, 2)),
            pltpu.SemaphoreType.DMA((n,)),
            pltpu.SemaphoreType.DMA((n,)),
            pltpu.SemaphoreType.DMA((n, 2)),
            pltpu.SemaphoreType.REGULAR,
            pltpu.SemaphoreType.REGULAR((n,)),
        ],
        compiler_params=pltpu.CompilerParams(collective_id=0, has_side_effects=True),
    )(
        layer_input,
        input_gain.reshape(1, width),
        key_weight,
        value_weight,
        stick_offsets,
        head_bias,
        queries,
    )


def solution(mesh):
    placed = (
        P(("grp", "tp"), "sp", None),
        P(),
        P(),
        P(),
        P(None, ("grp", "tp"), "sp"),
        P(),
        P(("grp", "tp"), "sp", None),
    )
    return jax.shard_map(
        shards,
        mesh=mesh,
        in_specs=placed,
        out_specs=(
            P(("grp", "tp"), "sp", None, None),
            P(("grp", "tp"), "sp", None, None),
            P(("grp", "tp"), "sp", None),
            P(("grp", "tp"), "sp", None),
        ),
        check_vma=False,
    )
```

time: 224 us -> 172 us (0.77)
  the two profiles are of different devices: /device:TPU:36 before, /device:TPU:800 now
where the time goes in v1:
time: 172 us; the launch traced here: 169 us
  Pallas kernels  163 us (95%)
  local copies, waits for them, and re-layouts  5.11 us (3%)
    pallas_call x1, Pallas kernels, shards(): pl.pallas_call(functools.partial(kernel, n), out_shape=(jax.ShapeDtypeStr...  163 us
    unnamed x10, local copies, waits for them, and re-layouts  5.11 us

profile of v1, /device:TPU:800, one launch (start us, length us, event | category | flops | bytes accessed | tf_op | source)
XLA Modules:
  0.0 169.1 jit_solution(11548481114049581746)
XLA Ops:
  0.6 163.4 %shard_map.102 = (bf16[1,1,6144,128]{3,2,1,0:T(8,128)(2,1)}, bf16[1,1,6144,128]{3,2,1,0:T(8,128)(2,1)}, bf16[1,1,6144]{2,1,0:T(2,128)(2,1)}, bf16[1,1,512]{2,1,0:T(2,128)(2,1)}) custom-call(bf16[4,384,2048]{2,1,0:T(8,128)(2,1)} %x_ref.1, f32[1,2048]{1,0:T(1,128)} %bitcast.1, bf16[2048,512]{1,0:T(8,128)(2,1)} %wk_ref.1, bf16[2048,512]{1,0:T(8,128)(2,1)} %wv_ref.1, ...), custom_call_target="tpu_custom_call" | custom-call | tf_op jit(solution)/shard_map/pallas_call | solution.py:234
  164.0 0.0 copy-start
  164.0 2.8 %copy.15 = bf16[1,1,6144,128]{3,2,1,0:T(8,128)(2,1)} copy(bf16[1,1,6144,128]{3,2,1,0:T(8,128)(2,1)} %get-tuple-element.8) | data formatting | bytes 3145728
  166.8 0.0 copy-done
  166.8 0.0 copy-start.1
  166.8 0.0 copy-start.2
  166.8 1.1 copy.16
  167.9 0.0 copy-done.1
  167.9 0.6 copy.17
  168.5 0.0 copy-done.2
  168.6 0.6 copy.18
Async XLA Ops:
  164.0 2.8 %copy-start = (bf16[1,1,6144,128]{3,2,1,0:T(8,128)(2,1)S(1)}, bf16[1,1,6144,128]{3,2,1,0:T(8,128)(2,1)}, u32[]{:S(2)}) copy-start(bf16[1,1,6144,128]{3,2,1,0:T(8,128)(2,1)} %get-tuple-element.9) | copy-start | bytes 4718596
  166.8 1.1 copy-start.1
  166.8 1.8 %copy-start.2 = (bf16[1,1,512]{2,1,0:T(2,128)(2,1)S(1)}, bf16[1,1,512]{2,1,0:T(2,128)(2,1)}, u32[]{:S(2)}) copy-start(bf16[1,1,512]{2,1,0:T(2,128)(2,1)} %get-tuple-element.11) | copy-start | bytes 3076

commit v2 on v1

v2 whole, which is shorter than its diff:
```python
import functools
import math

import jax
import jax.numpy as jnp
from jax import lax
from jax.experimental import pallas as pl
from jax.experimental.pallas import tpu as pltpu
from jax.sharding import PartitionSpec as P

H = 16
KVH = 4
HD = 128
EPSILON = 1e-06
MESH = pl.DeviceIdType.MESH
NORM_ROWS = 16
VMEM_LIMIT = 40 * 2**20


def split_rows(row, count):
    return [row[:, k * HD : (k + 1) * HD] for k in range(count)]


def kernel(
    n,
    x_ref, gain_hbm, wk_ref, wv_ref, off_hbm, bias_hbm, q_hbm,
    key_ref, value_ref, off_out_ref, read_ref,
    gain_ref, off_ref, bias_ref, q_ref, small_sem, x_buf, w_buf, normed, sent, relayed, off_sent, off_held, later, mixes, totals,
    x_sem, w_sem, send_sem, recv_sem, off_send_sem, off_recv_sem, relay_send_sem, relay_recv_sem, ready,
):
    prompts, block, _ = x_ref.shape
    group = H // KVH
    lane_rows = block // HD
    me = lax.axis_index("sp")
    barrier = pltpu.get_barrier_semaphore()

    def x_copy(i):
        return pltpu.make_async_copy(x_ref.at[i], x_buf.at[i], x_sem.at[i])

    def w_copies(h):
        columns = pl.ds(h * HD, HD)
        return (
            pltpu.make_async_copy(wk_ref.at[:, columns], w_buf.at[h, :, pl.ds(0, HD)], w_sem.at[h, 0]),
            pltpu.make_async_copy(wv_ref.at[:, columns], w_buf.at[h, :, pl.ds(HD, HD)], w_sem.at[h, 1]),
        )

    small = [
        pltpu.make_async_copy(source, target, small_sem.at[k])
        for k, (source, target) in enumerate(
            ((off_hbm, off_ref), (gain_hbm, gain_ref), (bias_hbm, bias_ref), (q_hbm, q_ref))
        )
    ]
    x_copy(0).start()
    for copy in small:
        copy.start()
    for h in range(KVH):
        for copy in w_copies(h):
            copy.start()
    for i in range(1, prompts):
        x_copy(i).start()

    @pl.when(me > 0)
    def _():
        pl.semaphore_wait(barrier, 1)

    @pl.when(me < n - 1)
    def _():
        pl.semaphore_signal(barrier, inc=1, device_id={"sp": lax.rem(me + 1, n)}, device_id_type=MESH)

    def announce(t, carry):
        pl.semaphore_signal(ready.at[me], inc=1, device_id={"sp": t}, device_id_type=MESH)
        return carry

    lax.fori_loop(0, me, announce, 0)

    for copy in small:
        copy.wait()
    for h in range(KVH):
        rows = off_ref[h].astype(jnp.float32)
        for i in range(prompts):
            pieces = split_rows(rows[i : i + 1], lane_rows)
            off_sent[i * KVH + h] = jnp.concatenate(pieces + pieces[:1], axis=0).astype(jnp.bfloat16)

    half, quarter = n // 2, n // 4
    from_low = jnp.logical_and(me < quarter, lax.rem(me, 2) == 1)
    from_high = jnp.logical_and(me >= n - quarter, lax.rem(me, 2) == 0)
    relays_low = jnp.logical_and(jnp.logical_and(me >= quarter, me < half), lax.rem(me, 2) == 1)
    relays_high = jnp.logical_and(jnp.logical_and(me >= half, me < n - quarter), lax.rem(me, 2) == 0)
    by_relay = jnp.logical_or(from_low, from_high)
    relays = jnp.logical_or(relays_low, relays_high)
    opposite = lax.rem(me + half, n)
    step = jnp.where(me < half, quarter, n - quarter)
    onward = lax.rem(me + step, n)
    origin = lax.rem(me - step + n, n)

    caches = (key_ref, value_ref)

    def place(kv, slot):
        return caches[kv].at[0, 0, pl.ds(pl.multiple_of(slot * block, block), block), :]

    def block_copy(kv, t, slot):
        return pltpu.make_async_remote_copy(
            sent.at[t, kv], place(kv, slot), send_sem.at[t, kv], recv_sem.at[slot, kv], device_id={"sp": t}, device_id_type=MESH
        )

    def off_copy(t, slot):
        return pltpu.make_async_remote_copy(
            off_sent.at[t], off_held.at[slot], off_send_sem.at[t], off_recv_sem.at[slot], device_id={"sp": t}, device_id_type=MESH
        )

    def relay_copy(kv):
        return pltpu.make_async_remote_copy(
            sent.at[opposite, kv], relayed.at[kv], send_sem.at[opposite, kv], relay_recv_sem.at[kv],
            device_id={"sp": onward}, device_id_type=MESH,
        )

    def onward_copy(kv):
        return pltpu.make_async_remote_copy(
            relayed.at[kv], place(kv, origin), relay_send_sem.at[kv], recv_sem.at[origin, kv],
            device_id={"sp": onward}, device_id_type=MESH,
        )

    def send(t):
        off_copy(t, me).start()
        through = jnp.logical_and(by_relay, t == opposite)

        @pl.when(through)
        def _():
            for kv in range(2):
                relay_copy(kv).start()

        @pl.when(jnp.logical_not(through))
        def _():
            for kv in range(2):
                block_copy(kv, t, me).start()

    def project_prompt(i, carry):
        x_copy(i).wait()

        def norm(r, carry):
            rows = pl.ds(pl.multiple_of(r * NORM_ROWS, NORM_ROWS), NORM_ROWS)
            x = x_buf[i, rows, :].astype(jnp.float32)
            scale = lax.rsqrt(jnp.mean(x * x, axis=-1, keepdims=True) + EPSILON)
            normed[rows, :] = (x * scale * gain_ref[...]).astype(jnp.bfloat16)
            return carry

        lax.fori_loop(0, block // NORM_ROWS, norm, 0)

        def project_head(h, carry):
            t = i * KVH + h

            @pl.when(i == 0)
            def _():
                for copy in w_copies(h):
                    copy.wait()

            rows = jnp.dot(normed[...], w_buf[h], preferred_element_type=jnp.float32).astype(jnp.bfloat16)

            @pl.when(t != me)
            def _():
                sent[t, 0] = rows[:, :HD]
                sent[t, 1] = rows[:, HD:]

            @pl.when(t == me)
            def _():
                own = pl.ds(pl.multiple_of(me * block, block), block)
                key_ref[0, 0, own, :] = rows[:, :HD]
                value_ref[0, 0, own, :] = rows[:, HD:]
                off_held[me] = off_sent[t]

            @pl.when(jnp.logical_and(t >= 1, t - 1 < me))
            def _():
                send(t - 1)

            return carry

        lax.fori_loop(0, KVH, project_head, 0)
        return carry

    lax.fori_loop(0, prompts, project_prompt, 0)

    def send_later(t, carry):
        pl.semaphore_wait(ready.at[t], 1)
        send(t)
        return carry

    lax.fori_loop(me + 1, n, send_later, 0)

    @pl.when(relays)
    def _():
        for kv in range(2):
            relay_copy(kv).wait_recv()
            onward_copy(kv).start()

    below = lax.broadcasted_iota(jnp.int32, (block, block), 0)
    across = lax.broadcasted_iota(jnp.int32, (block, block), 1)
    later[...] = jnp.where(below > across, 1.0, 0.0).astype(jnp.bfloat16)

    head = lax.rem(me, KVH)
    row_index = lax.broadcasted_iota(jnp.int32, (2 * group, 1), 0)
    query_rows = split_rows(q_ref[0], group)
    query = jnp.concatenate(query_rows + query_rows, axis=0)
    bias = jnp.zeros((2 * group, 1), jnp.float32)
    for g in range(group):
        bias = jnp.where(lax.rem(row_index, group) == g, bias_ref[head * group + g], bias)

    def read_block(j, carry):
        slot = lax.rem(me + j, n)

        @pl.when(j > 0)
        def _():
            off_copy(slot, slot).wait_recv()
            for kv in range(2):
                block_copy(kv, slot, slot).wait_recv()

        rows = pl.ds(pl.multiple_of(slot * block, block), block)
        off_rows = off_held[slot].astype(jnp.float32)
        off_row = jnp.concatenate([off_rows[k : k + 1] for k in range(lane_rows)], axis=1)
        off_out_ref[0, :, pl.ds(pl.multiple_of(slot * block, HD), block)] = off_row.astype(jnp.bfloat16)
        scores = lax.dot_general(query, key_ref[0, 0, rows, :], (((1,), (1,)), ((), ())), preferred_element_type=jnp.float32)
        scores = scores * (1.0 / math.sqrt(HD)) + bias + off_row
        tail = jnp.log1p(jnp.exp(-jnp.abs(scores)))
        spread = jnp.maximum(scores, 0.0) + tail
        log_take = jnp.minimum(scores, 0.0) - tail
        high = spread.astype(jnp.bfloat16)
        rest = spread - high.astype(jnp.float32)
        middle = rest.astype(jnp.bfloat16)
        low = (rest - middle.astype(jnp.float32)).astype(jnp.bfloat16)
        inside = (
            jnp.dot(high, later[...], preferred_element_type=jnp.float32)
            + jnp.dot(middle, later[...], preferred_element_type=jnp.float32)
            + jnp.dot(low, later[...], preferred_element_type=jnp.float32)
        )
        weights = jnp.exp(log_take - inside)
        coarse = weights.astype(jnp.bfloat16)
        fine = (weights - coarse.astype(jnp.float32)).astype(jnp.bfloat16)
        both = jnp.where(row_index < group, coarse.astype(jnp.float32), fine.astype(jnp.float32)).astype(jnp.bfloat16)
        mixes[slot] = jnp.dot(both, value_ref[0, 0, rows, :], preferred_element_type=jnp.float32)
        totals[slot] = jnp.broadcast_to(jnp.sum(spread, axis=-1, keepdims=True), (2 * group, HD))
        return carry

    lax.fori_loop(0, n, read_block, 0)

    def fold(j, carry):
        mixture, beyond = carry
        slot = n - 1 - j
        return mixture + jnp.exp(-beyond) * mixes[slot], beyond + totals[slot]

    zeros = jnp.zeros((2 * group, HD), jnp.float32)
    mixture, _ = lax.fori_loop(0, n, fold, (zeros, zeros))
    mixture = mixture[:group] + mixture[group:]
    mixture = mixture * lax.rsqrt(jnp.mean(mixture * mixture, axis=-1, keepdims=True) + EPSILON)
    read_ref[0] = jnp.concatenate([mixture[g : g + 1] for g in range(group)], axis=1).astype(jnp.bfloat16)

    def finish(j, carry):
        slot = lax.rem(me + j, n)

        @pl.when(j > 0)
        def _():
            off_copy(slot, slot).wait_send()
            for kv in range(2):
                block_copy(kv, slot, slot).wait_send()

        return carry

    lax.fori_loop(0, n, finish, 0)

    @pl.when(relays)
    def _():
        for kv in range(2):
            onward_copy(kv).wait_send()


def store_kernel(key_ref, value_ref, off_ref, read_ref, key_out, value_out, off_out, read_out, sems):
    copies = [
        pltpu.make_async_copy(source, target, sems.at[k])
        for k, (source, target) in enumerate(
            ((key_ref, key_out), (value_ref, value_out), (off_ref, off_out), (read_ref, read_out))
        )
    ]
    for copy in copies:
        copy.start()
    for copy in copies:
        copy.wait()


def shards(layer_input, input_gain, key_weight, value_weight, stick_offsets, head_bias, queries):
    seq_count, block, width = layer_input.shape
    n = lax.axis_size("sp")
    length = n * block
    group = H // KVH
    hbm = pl.BlockSpec(memory_space=pl.ANY)
    vmem = pl.BlockSpec(memory_space=pltpu.VMEM)
    smem = pl.BlockSpec(memory_space=pltpu.SMEM)
    shapes = ((1, 1, length, HD), (1, 1, length, HD), (1, 1, length), (1, 1, group * HD))
    arrived = pl.pallas_call(
        functools.partial(kernel, n),
        out_shape=tuple(pltpu.VMEM(shape, jnp.bfloat16) for shape in shapes),
        in_specs=[hbm] * 7,
        out_specs=(vmem, vmem, vmem, vmem),
        scratch_shapes=[
            pltpu.VMEM((1, width), jnp.float32),
            pltpu.VMEM(stick_offsets.shape, jnp.bfloat16),
            pltpu.SMEM(head_bias.shape, jnp.float32),
            pltpu.VMEM(queries.shape, jnp.bfloat16),
            pltpu.SemaphoreType.DMA((4,)),
            pltpu.VMEM((seq_count, block, width), jnp.bfloat16),
            pltpu.VMEM((KVH, width, 2 * HD), jnp.bfloat16),
            pltpu.VMEM((block, width), jnp.bfloat16),
            pltpu.VMEM((n, 2, block, HD), jnp.bfloat16),
            pltpu.VMEM((2, block, HD), jnp.bfloat16),
            pltpu.VMEM((n, 4, HD), jnp.bfloat16),
            pltpu.VMEM((n, 4, HD), jnp.bfloat16),
            pltpu.VMEM((block, block), jnp.bfloat16),
            pltpu.VMEM((n, 2 * group, HD), jnp.float32),
            pltpu.VMEM((n, 2 * group, HD), jnp.float32),
            pltpu.SemaphoreType.DMA((seq_count,)),
            pltpu.SemaphoreType.DMA((KVH, 2)),
            pltpu.SemaphoreType.DMA((n, 2)),
            pltpu.SemaphoreType.DMA((n, 2)),
            pltpu.SemaphoreType.DMA((n,)),
            pltpu.SemaphoreType.DMA((n,)),
            pltpu.SemaphoreType.DMA((2,)),
            pltpu.SemaphoreType.DMA((2,)),
            pltpu.SemaphoreType.REGULAR((n,)),
        ],
        compiler_params=pltpu.CompilerParams(collective_id=0, has_side_effects=True, vmem_limit_bytes=VMEM_LIMIT),
    )(
        *(
            pltpu.with_memory_space_constraint(array, pltpu.HBM)
            for array in (layer_input, input_gain.reshape(1, width), key_weight, value_weight, stick_offsets, head_bias, queries)
        )
    )
    return pl.pallas_call(
        store_kernel,
        out_shape=tuple(jax.ShapeDtypeStruct(shape, jnp.bfloat16) for shape in shapes),
        in_specs=[vmem] * 4,
        out_specs=(hbm,) * 4,
        scratch_shapes=[pltpu.SemaphoreType.DMA((4,))],
        compiler_params=pltpu.CompilerParams(vmem_limit_bytes=2**20),
    )(*arrived)


def solution(mesh):
    placed = (
        P(("grp", "tp"), "sp", None),
        P(),
        P(),
        P(),
        P(None, ("grp", "tp"), "sp"),
        P(),
        P(("grp", "tp"), "sp", None),
    )
    return jax.shard_map(
        shards,
        mesh=mesh,
        in_specs=placed,
        out_specs=(
            P(("grp", "tp"), "sp", None, None),
            P(("grp", "tp"), "sp", None, None),
            P(("grp", "tp"), "sp", None),
            P(("grp", "tp"), "sp", None),
        ),
        check_vma=False,
    )
```

time: 172 us -> 178 us (1.035)
  the two profiles are of different devices: /device:TPU:800 before, /device:TPU:1444 now
where the time goes in v2:
time: 178 us
  Pallas kernels  177 us (99%)
    pallas_call x1, Pallas kernels, shards(): pl.pallas_call(functools.partial(kernel, n), out_shape=tuple((pltpu.VMEM(...  175 us

profile of v2, /device:TPU:1444, one launch (start us, length us, event | category | flops | bytes accessed | tf_op | source)
XLA Modules:
  0.0 177.6 jit_solution(7711091833208403052)
XLA Ops:
  0.6 175.3 %shard_map.102 = (bf16[1,1,6144,128]{3,2,1,0:T(8,128)(2,1)S(1)}, bf16[1,1,6144,128]{3,2,1,0:T(8,128)(2,1)S(1)}, bf16[1,1,6144]{2,1,0:T(2,128)(2,1)S(1)}, bf16[1,1,512]{2,1,0:T(2,128)(2,1)S(1)}) custom-call(bf16[4,384,2048]{2,1,0:T(8,128)(2,1)} %x_ref.1, f32[1,2048]{1,0:T(1,128)} %bitcast.1, bf16[2048,512]{1,0:T(8,128)(2,1)} %wk_ref.1, ...), custom_call_target="tpu_custom_call" | custom-call | tf_op jit(solution)/shard_map/pallas_call | solution.py:296
  175.9 1.7 shard_map.103

commit v3 on v2

--- a/solution.py
+++ b/solution.py
@@ -13,7 +13,9 @@
 HD = 128
 EPSILON = 1e-06
 MESH = pl.DeviceIdType.MESH
-NORM_ROWS = 16
+NORM_ROWS = 128
+FOLD_ROWS = 256
+TIE_TURN = 11
 VMEM_LIMIT = 40 * 2**20
 
 
@@ -25,10 +27,10 @@
     n,
     x_ref, gain_hbm, wk_ref, wv_ref, off_hbm, bias_hbm, q_hbm,
     key_ref, value_ref, off_out_ref, read_ref,
-    gain_ref, off_ref, bias_ref, q_ref, small_sem, x_buf, w_buf, normed, sent, relayed, off_sent, off_held, later, mixes, totals,
-    x_sem, w_sem, send_sem, recv_sem, off_send_sem, off_recv_sem, relay_send_sem, relay_recv_sem, ready,
+    gain_ref, off_ref, bias_ref, q_ref, small_sem, x_buf, w_in, w_buf, gain_rows, scales, sent, off_sent, off_held, later, mixes, totals,
+    x_sem, w_sem, send_sem, recv_sem, off_send_sem, off_recv_sem, ready,
 ):
-    prompts, block, _ = x_ref.shape
+    prompts, block, width = x_ref.shape
     group = H // KVH
     lane_rows = block // HD
     me = lax.axis_index("sp")
@@ -40,8 +42,8 @@
     def w_copies(h):
         columns = pl.ds(h * HD, HD)
         return (
-            pltpu.make_async_copy(wk_ref.at[:, columns], w_buf.at[h, :, pl.ds(0, HD)], w_sem.at[h, 0]),
-            pltpu.make_async_copy(wv_ref.at[:, columns], w_buf.at[h, :, pl.ds(HD, HD)], w_sem.at[h, 1]),
+            pltpu.make_async_copy(wk_ref.at[:, columns], w_in.at[h, :, pl.ds(0, HD)], w_sem.at[h, 0]),
+            pltpu.make_async_copy(wv_ref.at[:, columns], w_in.at[h, :, pl.ds(HD, HD)], w_sem.at[h, 1]),
         )
 
     small = [
@@ -75,24 +77,16 @@
 
     for copy in small:
         copy.wait()
+    for k in range(width // HD):
+        columns = jnp.broadcast_to(gain_ref[:, k * HD : (k + 1) * HD], (HD, HD))
+        gain_rows[k * HD : (k + 1) * HD, :] = columns.T
     for h in range(KVH):
         rows = off_ref[h].astype(jnp.float32)
         for i in range(prompts):
             pieces = split_rows(rows[i : i + 1], lane_rows)
             off_sent[i * KVH + h] = jnp.concatenate(pieces + pieces[:1], axis=0).astype(jnp.bfloat16)
 
-    half, quarter = n // 2, n // 4
-    from_low = jnp.logical_and(me < quarter, lax.rem(me, 2) == 1)
-    from_high = jnp.logical_and(me >= n - quarter, lax.rem(me, 2) == 0)
-    relays_low = jnp.logical_and(jnp.logical_and(me >= quarter, me < half), lax.rem(me, 2) == 1)
-    relays_high = jnp.logical_and(jnp.logical_and(me >= half, me < n - quarter), lax.rem(me, 2) == 0)
-    by_relay = jnp.logical_or(from_low, from_high)
-    relays = jnp.logical_or(relays_low, relays_high)
-    opposite = lax.rem(me + half, n)
-    step = jnp.where(me < half, quarter, n - quarter)
-    onward = lax.rem(me + step, n)
-    origin = lax.rem(me - step + n, n)
-
+    half = n // 2
     caches = (key_ref, value_ref)
 
     def place(kv, slot):
@@ -108,69 +102,70 @@
             off_sent.at[t], off_held.at[slot], off_send_sem.at[t], off_recv_sem.at[slot], device_id={"sp": t}, device_id_type=MESH
         )
 
-    def relay_copy(kv):
-        return pltpu.make_async_remote_copy(
-            sent.at[opposite, kv], relayed.at[kv], send_sem.at[opposite, kv], relay_recv_sem.at[kv],
-            device_id={"sp": onward}, device_id_type=MESH,
-        )
-
-    def onward_copy(kv):
-        return pltpu.make_async_remote_copy(
-            relayed.at[kv], place(kv, origin), relay_send_sem.at[kv], recv_sem.at[origin, kv],
-            device_id={"sp": onward}, device_id_type=MESH,
-        )
-
     def send(t):
         off_copy(t, me).start()
-        through = jnp.logical_and(by_relay, t == opposite)
-
-        @pl.when(through)
-        def _():
+        for kv in range(2):
+            block_copy(kv, t, me).start()
+
+    def fold_gain(h):
+        for copy in w_copies(h):
+            copy.wait()
+
+        def fold_rows(r, carry):
+            rows = pl.ds(pl.multiple_of(r * FOLD_ROWS, FOLD_ROWS), FOLD_ROWS)
+            gain = gain_rows[rows, :]
             for kv in range(2):
-                relay_copy(kv).start()
-
-        @pl.when(jnp.logical_not(through))
-        def _():
-            for kv in range(2):
-                block_copy(kv, t, me).start()
+                columns = pl.ds(kv * HD, HD)
+                w_buf[h, rows, columns] = (w_in[h, rows, columns].astype(jnp.float32) * gain).astype(jnp.bfloat16)
+            return carry
+
+        lax.fori_loop(0, width // FOLD_ROWS, fold_rows, 0)
+
+    def measure_rows(i):
+        x_copy(i).wait()
+
+        def measure(r, carry):
+            rows = pl.ds(pl.multiple_of(r * NORM_ROWS, NORM_ROWS), NORM_ROWS)
+            squares = jnp.zeros((NORM_ROWS, HD), jnp.float32)
+            for k in range(width // HD):
+                x = x_buf[i, rows, pl.ds(k * HD, HD)].astype(jnp.float32)
+                squares += x * x
+            mean = jnp.sum(squares, axis=-1, keepdims=True) * (1.0 / width)
+            scales[rows, :] = jnp.broadcast_to(lax.rsqrt(mean + EPSILON), (NORM_ROWS, HD))
+            return carry
+
+        lax.fori_loop(0, block // NORM_ROWS, measure, 0)
 
     def project_prompt(i, carry):
-        x_copy(i).wait()
-
-        def norm(r, carry):
-            rows = pl.ds(pl.multiple_of(r * NORM_ROWS, NORM_ROWS), NORM_ROWS)
-            x = x_buf[i, rows, :].astype(jnp.float32)
-            scale = lax.rsqrt(jnp.mean(x * x, axis=-1, keepdims=True) + EPSILON)
-            normed[rows, :] = (x * scale * gain_ref[...]).astype(jnp.bfloat16)
-            return carry
-
-        lax.fori_loop(0, block // NORM_ROWS, norm, 0)
+        measure_rows(i)
 
         def project_head(h, carry):
             t = i * KVH + h
 
             @pl.when(i == 0)
             def _():
-                for copy in w_copies(h):
-                    copy.wait()
-
-            rows = jnp.dot(normed[...], w_buf[h], preferred_element_type=jnp.float32).astype(jnp.bfloat16)
+                fold_gain(h)
+
+            rows = jnp.dot(x_buf[i], w_buf[h], preferred_element_type=jnp.float32)
+            scale = scales[...]
+            keys = (rows[:, :HD] * scale).astype(jnp.bfloat16)
+            values = (rows[:, HD:] * scale).astype(jnp.bfloat16)
 
             @pl.when(t != me)
             def _():
-                sent[t, 0] = rows[:, :HD]
-                sent[t, 1] = rows[:, HD:]
+                sent[t, 0] = keys
+                sent[t, 1] = values
 
             @pl.when(t == me)
             def _():
                 own = pl.ds(pl.multiple_of(me * block, block), block)
-                key_ref[0, 0, own, :] = rows[:, :HD]
-                value_ref[0, 0, own, :] = rows[:, HD:]
+                key_ref[0, 0, own, :] = keys
+                value_ref[0, 0, own, :] = values
                 off_held[me] = off_sent[t]
 
-            @pl.when(jnp.logical_and(t >= 1, t - 1 < me))
+            @pl.when(t < me)
             def _():
-                send(t - 1)
+                send(t)
 
             return carry
 
@@ -185,12 +180,6 @@
         return carry
 
     lax.fori_loop(me + 1, n, send_later, 0)
-
-    @pl.when(relays)
-    def _():
-        for kv in range(2):
-            relay_copy(kv).wait_recv()
-            onward_copy(kv).start()
 
     below = lax.broadcasted_iota(jnp.int32, (block, block), 0)
     across = lax.broadcasted_iota(jnp.int32, (block, block), 1)
@@ -204,8 +193,14 @@
     for g in range(group):
         bias = jnp.where(lax.rem(row_index, group) == g, bias_ref[head * group + g], bias)
 
+    def source(j):
+        k = jnp.where(j > TIE_TURN, j - 2, j - 1)
+        away = jnp.where(lax.rem(k, 2) == 0, half - 1 - k // 2, n - 1 - k // 2)
+        away = jnp.where(j == TIE_TURN, half, away)
+        return lax.rem(me + jnp.where(j == 0, 0, away), n)
+
     def read_block(j, carry):
-        slot = lax.rem(me + j, n)
+        slot = source(j)
 
         @pl.when(j > 0)
         def _():
@@ -226,11 +221,9 @@
         rest = spread - high.astype(jnp.float32)
         middle = rest.astype(jnp.bfloat16)
         low = (rest - middle.astype(jnp.float32)).astype(jnp.bfloat16)
-        inside = (
-            jnp.dot(high, later[...], preferred_element_type=jnp.float32)
-            + jnp.dot(middle, later[...], preferred_element_type=jnp.float32)
-            + jnp.dot(low, later[...], preferred_element_type=jnp.float32)
-        )
+        parts = jnp.concatenate([part.astype(jnp.float32) for part in (high, middle, low)], axis=0).astype(jnp.bfloat16)
+        sums = jnp.dot(parts, later[...], preferred_element_type=jnp.float32)
+        inside = sums[: 2 * group] + sums[2 * group : 4 * group] + sums[4 * group :]
         weights = jnp.exp(log_take - inside)
         coarse = weights.astype(jnp.bfloat16)
         fine = (weights - coarse.astype(jnp.float32)).astype(jnp.bfloat16)
@@ -264,11 +257,6 @@
         return carry
 
     lax.fori_loop(0, n, finish, 0)
-
-    @pl.when(relays)
-    def _():
-        for kv in range(2):
-            onward_copy(kv).wait_send()
 
 
 def store_kernel(key_ref, value_ref, off_ref, read_ref, key_out, value_out, off_out, read_out, sems):
@@ -306,9 +294,10 @@
             pltpu.SemaphoreType.DMA((4,)),
             pltpu.VMEM((seq_count, block, width), jnp.bfloat16),
             pltpu.VMEM((KVH, width, 2 * HD), jnp.bfloat16),
-            pltpu.VMEM((block, width), jnp.bfloat16),
+            pltpu.VMEM((KVH, width, 2 * HD), jnp.bfloat16),
+            pltpu.VMEM((width, HD), jnp.float32),
+            pltpu.VMEM((block, HD), jnp.float32),
             pltpu.VMEM((n, 2, block, HD), jnp.bfloat16),
-            pltpu.VMEM((2, block, HD), jnp.bfloat16),
             pltpu.VMEM((n, 4, HD), jnp.bfloat16),
             pltpu.VMEM((n, 4, HD), jnp.bfloat16),
             pltpu.VMEM((block, block), jnp.bfloat16),
@@ -320,8 +309,6 @@
             pltpu.SemaphoreType.DMA((n, 2)),
             pltpu.SemaphoreType.DMA((n,)),
             pltpu.SemaphoreType.DMA((n,)),
-            pltpu.SemaphoreType.DMA((2,)),
-            pltpu.SemaphoreType.DMA((2,)),
             pltpu.SemaphoreType.REGULAR((n,)),
         ],
         compiler_params=pltpu.CompilerParams(collective_id=0, has_side_effects=True, vmem_limit_bytes=VMEM_LIMIT),

time: 178 us -> 161 us (0.904)
  the two profiles are of different devices: /device:TPU:1444 before, /device:TPU:800 now
where the time goes in v3:
time: 161 us; the launch traced here: 159 us
  Pallas kernels  158 us (98%)
    pallas_call x1, Pallas kernels, shards(): pl.pallas_call(functools.partial(kernel, n), out_shape=tuple((pltpu.VMEM(...  156 us

profile of v3, /device:TPU:800, one launch (start us, length us, event | category | flops | bytes accessed | tf_op | source)
XLA Modules:
  0.0 158.6 jit_solution(17290355605778487905)
XLA Ops:
  0.6 156.2 %shard_map.102 = (bf16[1,1,6144,128]{3,2,1,0:T(8,128)(2,1)S(1)}, bf16[1,1,6144,128]{3,2,1,0:T(8,128)(2,1)S(1)}, bf16[1,1,6144]{2,1,0:T(2,128)(2,1)S(1)}, bf16[1,1,512]{2,1,0:T(2,128)(2,1)S(1)}) custom-call(bf16[4,384,2048]{2,1,0:T(8,128)(2,1)} %x_ref.1, f32[1,2048]{1,0:T(1,128)} %bitcast.1, bf16[2048,512]{1,0:T(8,128)(2,1)} %wk_ref.1, ...), custom_call_target="tpu_custom_call" | custom-call | tf_op jit(solution)/shard_map/pallas_call | solution.py:284
  156.9 1.7 %shard_map.103 = (bf16[1,1,6144,128]{3,2,1,0:T(8,128)(2,1)}, bf16[1,1,6144,128]{3,2,1,0:T(8,128)(2,1)}, bf16[1,1,6144]{2,1,0:T(2,128)(2,1)}, bf16[1,1,512]{2,1,0:T(2,128)(2,1)}) custom-call(bf16[1,1,6144,128]{3,2,1,0:T(8,128)(2,1)S(1)} %get-tuple-element.8.key_ref, bf16[1,1,6144,128]{3,2,1,0:T(8,128)(2,1)S(1)} %get-tuple-element.9.value_ref, ...), custom_call_target="tpu_custom_call" | custom-call | tf_op jit(solution)/shard_map/pallas_call | solution.py:321

commit v4 on v3

--- a/solution.py
+++ b/solution.py
@@ -13,8 +13,6 @@
 HD = 128
 EPSILON = 1e-06
 MESH = pl.DeviceIdType.MESH
-NORM_ROWS = 128
-FOLD_ROWS = 256
 TIE_TURN = 11
 VMEM_LIMIT = 40 * 2**20
 
@@ -27,8 +25,8 @@
     n,
     x_ref, gain_hbm, wk_ref, wv_ref, off_hbm, bias_hbm, q_hbm,
     key_ref, value_ref, off_out_ref, read_ref,
-    gain_ref, off_ref, bias_ref, q_ref, small_sem, x_buf, w_in, w_buf, gain_rows, scales, sent, off_sent, off_held, later, mixes, totals,
-    x_sem, w_sem, send_sem, recv_sem, off_send_sem, off_recv_sem, ready,
+    gain_ref, off_ref, bias_ref, q_ref, small_sem, x_buf, w_in, w_buf, gain_rows, scales, sent, relayed, off_sent, off_held, later, mixes, totals,
+    x_sem, w_sem, send_sem, recv_sem, off_send_sem, off_recv_sem, relay_send_sem, relay_recv_sem, ready,
 ):
     prompts, block, width = x_ref.shape
     group = H // KVH
@@ -80,103 +78,144 @@
     for k in range(width // HD):
         columns = jnp.broadcast_to(gain_ref[:, k * HD : (k + 1) * HD], (HD, HD))
         gain_rows[k * HD : (k + 1) * HD, :] = columns.T
+    half, quarter = n // 2, n // 4
+    by_relay, relays = me == half, me == quarter
+    caches = (key_ref, value_ref)
+
+    def place(kv, slot):
+        return caches[kv].at[0, 0, pl.ds(pl.multiple_of(slot * block, block), block), :]
+
+    def block_copy(kv, t, slot):
+        return pltpu.make_async_remote_copy(
+            sent.at[t, kv], place(kv, slot), send_sem.at[t, kv], recv_sem.at[slot, kv], device_id={"sp": t}, device_id_type=MESH
+        )
+
+    def off_copy(t, slot):
+        return pltpu.make_async_remote_copy(
+            off_sent.at[t], off_held.at[slot], off_send_sem.at[t], off_recv_sem.at[slot], device_id={"sp": t}, device_id_type=MESH
+        )
+
+    def to_relay(kv):
+        return pltpu.make_async_remote_copy(
+            sent.at[0, kv], relayed.at[kv], send_sem.at[0, kv], relay_recv_sem.at[kv],
+            device_id={"sp": quarter}, device_id_type=MESH,
+        )
+
+    def from_relay(kv):
+        return pltpu.make_async_remote_copy(
+            relayed.at[kv], place(kv, half), relay_send_sem.at[kv], recv_sem.at[half, kv],
+            device_id={"sp": 0}, device_id_type=MESH,
+        )
+
+    def send(t):
+        through = jnp.logical_and(by_relay, t == 0)
+
+        @pl.when(through)
+        def _():
+            for kv in range(2):
+                to_relay(kv).start()
+
+        @pl.when(jnp.logical_not(through))
+        def _():
+            for kv in range(2):
+                block_copy(kv, t, me).start()
+
+    def fold_gain(h):
+        for kv in range(2):
+            columns = pl.ds(kv * HD, HD)
+            w_buf[h, :, columns] = (w_in[h, :, columns].astype(jnp.float32) * gain_rows[...]).astype(jnp.bfloat16)
+
+    def measure_rows(i, start, count):
+        rows = pl.ds(start, count)
+        squares = jnp.zeros((count, HD), jnp.float32)
+        for k in range(width // HD):
+            x = x_buf[i, rows, pl.ds(k * HD, HD)].astype(jnp.float32)
+            squares += x * x
+        mean = jnp.sum(squares, axis=-1, keepdims=True) * (1.0 / width)
+        scales[lax.rem(i, 2), rows, :] = jnp.broadcast_to(lax.rsqrt(mean + EPSILON), (count, HD))
+
+    def project_pair(i, pair):
+        for h in (2 * pair, 2 * pair + 1):
+            rows = jnp.dot(x_buf[i], w_buf[h], preferred_element_type=jnp.float32)
+            scale = scales[lax.rem(i, 2)]
+            for kv in range(2):
+                sent[i * KVH + h, kv] = (rows[:, kv * HD : (kv + 1) * HD] * scale).astype(jnp.bfloat16)
+
+    def hand_out(i, pair):
+        for h in (2 * pair, 2 * pair + 1):
+            t = i * KVH + h
+
+            @pl.when(t == me)
+            def _():
+                own = pl.ds(pl.multiple_of(me * block, block), block)
+                for kv in range(2):
+                    caches[kv][0, 0, own, :] = sent[t, kv]
+
+            @pl.when(t < me)
+            def _():
+                send(t)
+
     for h in range(KVH):
         rows = off_ref[h].astype(jnp.float32)
         for i in range(prompts):
             pieces = split_rows(rows[i : i + 1], lane_rows)
             off_sent[i * KVH + h] = jnp.concatenate(pieces + pieces[:1], axis=0).astype(jnp.bfloat16)
 
-    half = n // 2
-    caches = (key_ref, value_ref)
-
-    def place(kv, slot):
-        return caches[kv].at[0, 0, pl.ds(pl.multiple_of(slot * block, block), block), :]
-
-    def block_copy(kv, t, slot):
-        return pltpu.make_async_remote_copy(
-            sent.at[t, kv], place(kv, slot), send_sem.at[t, kv], recv_sem.at[slot, kv], device_id={"sp": t}, device_id_type=MESH
-        )
-
-    def off_copy(t, slot):
-        return pltpu.make_async_remote_copy(
-            off_sent.at[t], off_held.at[slot], off_send_sem.at[t], off_recv_sem.at[slot], device_id={"sp": t}, device_id_type=MESH
-        )
-
-    def send(t):
+    off_held[me] = off_sent[me]
+
+    def send_offsets(t, carry):
         off_copy(t, me).start()
-        for kv in range(2):
-            block_copy(kv, t, me).start()
-
-    def fold_gain(h):
+        return carry
+
+    lax.fori_loop(0, me, send_offsets, 0)
+
+    half_block = block // 2
+    for h in range(2):
         for copy in w_copies(h):
             copy.wait()
-
-        def fold_rows(r, carry):
-            rows = pl.ds(pl.multiple_of(r * FOLD_ROWS, FOLD_ROWS), FOLD_ROWS)
-            gain = gain_rows[rows, :]
-            for kv in range(2):
-                columns = pl.ds(kv * HD, HD)
-                w_buf[h, rows, columns] = (w_in[h, rows, columns].astype(jnp.float32) * gain).astype(jnp.bfloat16)
-            return carry
-
-        lax.fori_loop(0, width // FOLD_ROWS, fold_rows, 0)
-
-    def measure_rows(i):
-        x_copy(i).wait()
-
-        def measure(r, carry):
-            rows = pl.ds(pl.multiple_of(r * NORM_ROWS, NORM_ROWS), NORM_ROWS)
-            squares = jnp.zeros((NORM_ROWS, HD), jnp.float32)
-            for k in range(width // HD):
-                x = x_buf[i, rows, pl.ds(k * HD, HD)].astype(jnp.float32)
-                squares += x * x
-            mean = jnp.sum(squares, axis=-1, keepdims=True) * (1.0 / width)
-            scales[rows, :] = jnp.broadcast_to(lax.rsqrt(mean + EPSILON), (NORM_ROWS, HD))
-            return carry
-
-        lax.fori_loop(0, block // NORM_ROWS, measure, 0)
-
-    def project_prompt(i, carry):
-        measure_rows(i)
-
-        def project_head(h, carry):
-            t = i * KVH + h
-
-            @pl.when(i == 0)
-            def _():
-                fold_gain(h)
-
-            rows = jnp.dot(x_buf[i], w_buf[h], preferred_element_type=jnp.float32)
-            scale = scales[...]
-            keys = (rows[:, :HD] * scale).astype(jnp.bfloat16)
-            values = (rows[:, HD:] * scale).astype(jnp.bfloat16)
-
-            @pl.when(t != me)
-            def _():
-                sent[t, 0] = keys
-                sent[t, 1] = values
-
-            @pl.when(t == me)
-            def _():
-                own = pl.ds(pl.multiple_of(me * block, block), block)
-                key_ref[0, 0, own, :] = keys
-                value_ref[0, 0, own, :] = values
-                off_held[me] = off_sent[t]
-
-            @pl.when(t < me)
-            def _():
-                send(t)
-
-            return carry
-
-        lax.fori_loop(0, KVH, project_head, 0)
-        return carry
-
-    lax.fori_loop(0, prompts, project_prompt, 0)
+        fold_gain(h)
+    x_copy(0).wait()
+    for k in range(2):
+        measure_rows(0, k * half_block, half_block)
+
+    def project_prompt(i, first):
+        following = min(i + 1, prompts - 1) if first else jnp.minimum(i + 1, prompts - 1)
+        for pair in range(KVH // 2):
+            if first and pair == 0:
+                for h in range(2, KVH):
+                    for copy in w_copies(h):
+                        copy.wait()
+                    fold_gain(h)
+                x_copy(1).wait()
+            elif not first and pair == 0:
+
+                @pl.when(i < prompts - 1)
+                def _():
+                    x_copy(i + 1).wait()
+
+            project_pair(i, pair)
+            measure_rows(following, pair * half_block, half_block)
+            hand_out(i, pair)
+
+    project_prompt(0, True)
+
+    def project_rest(i, carry):
+        project_prompt(i, False)
+        return carry
+
+    lax.fori_loop(1, prompts, project_rest, 0)
 
     def send_later(t, carry):
         pl.semaphore_wait(ready.at[t], 1)
+        off_copy(t, me).start()
         send(t)
+
+        @pl.when(jnp.logical_and(relays, t == n - quarter))
+        def _():
+            for kv in range(2):
+                to_relay(kv).wait_recv()
+                from_relay(kv).start()
+
         return carry
 
     lax.fori_loop(me + 1, n, send_later, 0)
@@ -257,6 +296,11 @@
         return carry
 
     lax.fori_loop(0, n, finish, 0)
+
+    @pl.when(relays)
+    def _():
+        for kv in range(2):
+            from_relay(kv).wait_send()
 
 
 def store_kernel(key_ref, value_ref, off_ref, read_ref, key_out, value_out, off_out, read_out, sems):
@@ -296,8 +340,9 @@
             pltpu.VMEM((KVH, width, 2 * HD), jnp.bfloat16),
             pltpu.VMEM((KVH, width, 2 * HD), jnp.bfloat16),
             pltpu.VMEM((width, HD), jnp.float32),
-            pltpu.VMEM((block, HD), jnp.float32),
+            pltpu.VMEM((2, block, HD), jnp.float32),
             pltpu.VMEM((n, 2, block, HD), jnp.bfloat16),
+            pltpu.VMEM((2, block, HD), jnp.bfloat16),
             pltpu.VMEM((n, 4, HD), jnp.bfloat16),
             pltpu.VMEM((n, 4, HD), jnp.bfloat16),
             pltpu.VMEM((block, block), jnp.bfloat16),
@@ -309,6 +354,8 @@
             pltpu.SemaphoreType.DMA((n, 2)),
             pltpu.SemaphoreType.DMA((n,)),
             pltpu.SemaphoreType.DMA((n,)),
+            pltpu.SemaphoreType.DMA((2,)),
+            pltpu.SemaphoreType.DMA((2,)),
             pltpu.SemaphoreType.REGULAR((n,)),
         ],
         compiler_params=pltpu.CompilerParams(collective_id=0, has_side_effects=True, vmem_limit_bytes=VMEM_LIMIT),

time: 161 us -> 156 us (0.969); the launches traced: 159 us -> 156 us
  Pallas kernels: 158 us -> 155 us
    pallas_call x1, Pallas kernels: 156 us -> 153 us  [shards(): pl.pallas_call(functools.partial(kernel, n), out_shape=tuple((pltpu.VMEM(...]
where the time goes in v4:
time: 156 us
  Pallas kernels  155 us (99%)
    pallas_call x1, Pallas kernels, shards(): pl.pallas_call(functools.partial(kernel, n), out_shape=tuple((pltpu.VMEM(...  153 us

profile of v4, /device:TPU:800, one launch (start us, length us, event | category | flops | bytes accessed | tf_op | source)
XLA Modules:
  0.0 155.7 jit_solution(11111486508800654299)
XLA Ops:
  0.6 153.4 %shard_map.102 = (bf16[1,1,6144,128]{3,2,1,0:T(8,128)(2,1)S(1)}, bf16[1,1,6144,128]{3,2,1,0:T(8,128)(2,1)S(1)}, bf16[1,1,6144]{2,1,0:T(2,128)(2,1)S(1)}, bf16[1,1,512]{2,1,0:T(2,128)(2,1)S(1)}) custom-call(bf16[4,384,2048]{2,1,0:T(8,128)(2,1)} %x_ref.1, f32[1,2048]{1,0:T(1,128)} %bitcast.1, bf16[2048,512]{1,0:T(8,128)(2,1)} %wk_ref.1, ...), custom_call_target="tpu_custom_call" | custom-call | tf_op jit(solution)/shard_map/pallas_call | solution.py:328
  154.0 1.7 %shard_map.103 = (bf16[1,1,6144,128]{3,2,1,0:T(8,128)(2,1)}, bf16[1,1,6144,128]{3,2,1,0:T(8,128)(2,1)}, bf16[1,1,6144]{2,1,0:T(2,128)(2,1)}, bf16[1,1,512]{2,1,0:T(2,128)(2,1)}) custom-call(bf16[1,1,6144,128]{3,2,1,0:T(8,128)(2,1)S(1)} %get-tuple-element.8.key_ref, bf16[1,1,6144,128]{3,2,1,0:T(8,128)(2,1)S(1)} %get-tuple-element.9.value_ref, ...), custom_call_target="tpu_custom_call" | custom-call | tf_op jit(solution)/shard_map/pallas_call | solution.py:368

commit v5 on v4

--- a/solution.py
+++ b/solution.py
@@ -14,6 +14,7 @@
 EPSILON = 1e-06
 MESH = pl.DeviceIdType.MESH
 TIE_TURN = 11
+STORES = 4
 VMEM_LIMIT = 40 * 2**20
 
 
@@ -134,15 +135,15 @@
         mean = jnp.sum(squares, axis=-1, keepdims=True) * (1.0 / width)
         scales[lax.rem(i, 2), rows, :] = jnp.broadcast_to(lax.rsqrt(mean + EPSILON), (count, HD))
 
-    def project_pair(i, pair):
-        for h in (2 * pair, 2 * pair + 1):
+    def project_heads(i, heads):
+        for h in heads:
             rows = jnp.dot(x_buf[i], w_buf[h], preferred_element_type=jnp.float32)
             scale = scales[lax.rem(i, 2)]
             for kv in range(2):
                 sent[i * KVH + h, kv] = (rows[:, kv * HD : (kv + 1) * HD] * scale).astype(jnp.bfloat16)
 
-    def hand_out(i, pair):
-        for h in (2 * pair, 2 * pair + 1):
+    def hand_out(i, heads):
+        for h in heads:
             t = i * KVH + h
 
             @pl.when(t == me)
@@ -151,9 +152,36 @@
                 for kv in range(2):
                     caches[kv][0, 0, own, :] = sent[t, kv]
 
-            @pl.when(t < me)
+            @pl.when(t > me)
+            def _():
+                pl.semaphore_wait(ready.at[t], 1)
+                off_copy(t, me).start()
+
+            @pl.when(t != me)
             def _():
                 send(t)
+
+            @pl.when(jnp.logical_and(relays, t == n - quarter))
+            def _():
+                for kv in range(2):
+                    to_relay(kv).wait_recv()
+                    from_relay(kv).start()
+
+    half_block = block // 2
+
+    def wait_weights(h):
+        for copy in w_copies(h):
+            copy.wait()
+
+    wait_weights(0)
+    fold_gain(0)
+    wait_weights(1)
+    x_copy(0).wait()
+    for k in range(2):
+        measure_rows(0, k * half_block, half_block)
+    project_heads(0, (0,))
+    fold_gain(1)
+    hand_out(0, (0,))
 
     for h in range(KVH):
         rows = off_ref[h].astype(jnp.float32)
@@ -169,56 +197,36 @@
 
     lax.fori_loop(0, me, send_offsets, 0)
 
-    half_block = block // 2
-    for h in range(2):
-        for copy in w_copies(h):
-            copy.wait()
-        fold_gain(h)
-    x_copy(0).wait()
+    wait_weights(2)
+    wait_weights(3)
+    project_heads(0, (1,))
+    fold_gain(2)
+    fold_gain(3)
+    hand_out(0, (1,))
+    x_copy(1).wait()
+    project_heads(0, (2, 3))
     for k in range(2):
-        measure_rows(0, k * half_block, half_block)
-
-    def project_prompt(i, first):
-        following = min(i + 1, prompts - 1) if first else jnp.minimum(i + 1, prompts - 1)
+        measure_rows(1, k * half_block, half_block)
+    hand_out(0, (2, 3))
+
+    def project_prompt(i):
+        following = jnp.minimum(i + 1, prompts - 1)
+
+        @pl.when(i < prompts - 1)
+        def _():
+            x_copy(i + 1).wait()
+
         for pair in range(KVH // 2):
-            if first and pair == 0:
-                for h in range(2, KVH):
-                    for copy in w_copies(h):
-                        copy.wait()
-                    fold_gain(h)
-                x_copy(1).wait()
-            elif not first and pair == 0:
-
-                @pl.when(i < prompts - 1)
-                def _():
-                    x_copy(i + 1).wait()
-
-            project_pair(i, pair)
+            heads = (2 * pair, 2 * pair + 1)
+            project_heads(i, heads)
             measure_rows(following, pair * half_block, half_block)
-            hand_out(i, pair)
-
-    project_prompt(0, True)
+            hand_out(i, heads)
 
     def project_rest(i, carry):
-        project_prompt(i, False)
+        project_prompt(i)
         return carry
 
     lax.fori_loop(1, prompts, project_rest, 0)
-
-    def send_later(t, carry):
-        pl.semaphore_wait(ready.at[t], 1)
-        off_copy(t, me).start()
-        send(t)
-
-        @pl.when(jnp.logical_and(relays, t == n - quarter))
-        def _():
-            for kv in range(2):
-                to_relay(kv).wait_recv()
-                from_relay(kv).start()
-
-        return carry
-
-    lax.fori_loop(me + 1, n, send_later, 0)
 
     below = lax.broadcasted_iota(jnp.int32, (block, block), 0)
     across = lax.broadcasted_iota(jnp.int32, (block, block), 1)
@@ -279,7 +287,7 @@
         return mixture + jnp.exp(-beyond) * mixes[slot], beyond + totals[slot]
 
     zeros = jnp.zeros((2 * group, HD), jnp.float32)
-    mixture, _ = lax.fori_loop(0, n, fold, (zeros, zeros))
+    mixture, _ = lax.fori_loop(0, n, fold, (zeros, zeros), unroll=True)
     mixture = mixture[:group] + mixture[group:]
     mixture = mixture * lax.rsqrt(jnp.mean(mixture * mixture, axis=-1, keepdims=True) + EPSILON)
     read_ref[0] = jnp.concatenate([mixture[g : g + 1] for g in range(group)], axis=1).astype(jnp.bfloat16)
@@ -304,12 +312,13 @@
 
 
 def store_kernel(key_ref, value_ref, off_ref, read_ref, key_out, value_out, off_out, read_out, sems):
-    copies = [
-        pltpu.make_async_copy(source, target, sems.at[k])
-        for k, (source, target) in enumerate(
-            ((key_ref, key_out), (value_ref, value_out), (off_ref, off_out), (read_ref, read_out))
-        )
-    ]
+    pairs = [(off_ref, off_out), (read_ref, read_out)]
+    rows = key_ref.shape[2] // STORES
+    for k in range(STORES):
+        part = pl.ds(k * rows, rows)
+        for source, target in ((key_ref, key_out), (value_ref, value_out)):
+            pairs.append((source.at[0, 0, part, :], target.at[0, 0, part, :]))
+    copies = [pltpu.make_async_copy(source, target, sems.at[k]) for k, (source, target) in enumerate(pairs)]
     for copy in copies:
         copy.start()
     for copy in copies:
@@ -370,7 +379,7 @@
         out_shape=tuple(jax.ShapeDtypeStruct(shape, jnp.bfloat16) for shape in shapes),
         in_specs=[vmem] * 4,
         out_specs=(hbm,) * 4,
-        scratch_shapes=[pltpu.SemaphoreType.DMA((4,))],
+        scratch_shapes=[pltpu.SemaphoreType.DMA((2 * STORES + 2,))],
         compiler_params=pltpu.CompilerParams(vmem_limit_bytes=2**20),
     )(*arrived)
 

time: 156 us -> 156 us (level)
  no operation moved by 1% of the time
where the time goes in v5:
time: 156 us
  Pallas kernels  155 us (99%)
    pallas_call x1, Pallas kernels, shards(): pl.pallas_call(functools.partial(kernel, n), out_shape=tuple((pltpu.VMEM(...  153 us

profile of v5, /device:TPU:800, one launch (start us, length us, event | category | flops | bytes accessed | tf_op | source)
XLA Modules:
  0.0 155.6 jit_solution(6516909432851978040)
XLA Ops:
  0.6 153.2 %shard_map.102 = (bf16[1,1,6144,128]{3,2,1,0:T(8,128)(2,1)S(1)}, bf16[1,1,6144,128]{3,2,1,0:T(8,128)(2,1)S(1)}, bf16[1,1,6144]{2,1,0:T(2,128)(2,1)S(1)}, bf16[1,1,512]{2,1,0:T(2,128)(2,1)S(1)}) custom-call(bf16[4,384,2048]{2,1,0:T(8,128)(2,1)} %x_ref.1, f32[1,2048]{1,0:T(1,128)} %bitcast.1, bf16[2048,512]{1,0:T(8,128)(2,1)} %wk_ref.1, ...), custom_call_target="tpu_custom_call" | custom-call | tf_op jit(solution)/shard_map/pallas_call | solution.py:337
  153.9 1.8 %shard_map.103 = (bf16[1,1,6144,128]{3,2,1,0:T(8,128)(2,1)}, bf16[1,1,6144,128]{3,2,1,0:T(8,128)(2,1)}, bf16[1,1,6144]{2,1,0:T(2,128)(2,1)}, bf16[1,1,512]{2,1,0:T(2,128)(2,1)}) custom-call(bf16[1,1,6144,128]{3,2,1,0:T(8,128)(2,1)S(1)} %get-tuple-element.8.key_ref, bf16[1,1,6144,128]{3,2,1,0:T(8,128)(2,1)S(1)} %get-tuple-element.9.value_ref, ...), custom_call_target="tpu_custom_call" | custom-call | tf_op jit(solution)/shard_map/pallas_call | solution.py:377

commit v6 on v5

--- a/solution.py
+++ b/solution.py
@@ -25,9 +25,9 @@
 def kernel(
     n,
     x_ref, gain_hbm, wk_ref, wv_ref, off_hbm, bias_hbm, q_hbm,
-    key_ref, value_ref, off_out_ref, read_ref,
+    held, off_out_ref, read_ref,
     gain_ref, off_ref, bias_ref, q_ref, small_sem, x_buf, w_in, w_buf, gain_rows, scales, sent, relayed, off_sent, off_held, later, mixes, totals,
-    x_sem, w_sem, send_sem, recv_sem, off_send_sem, off_recv_sem, relay_send_sem, relay_recv_sem, ready,
+    x_sem, w_sem, send_sem, recv_sem, off_send_sem, off_recv_sem, relay_sem, ready,
 ):
     prompts, block, width = x_ref.shape
     group = H // KVH
@@ -51,14 +51,11 @@
             ((off_hbm, off_ref), (gain_hbm, gain_ref), (bias_hbm, bias_ref), (q_hbm, q_ref))
         )
     ]
-    x_copy(0).start()
     for copy in small:
         copy.start()
-    for h in range(KVH):
-        for copy in w_copies(h):
-            copy.start()
-    for i in range(1, prompts):
-        x_copy(i).start()
+    for copy in w_copies(0):
+        copy.start()
+    x_copy(0).start()
 
     @pl.when(me > 0)
     def _():
@@ -81,14 +78,9 @@
         gain_rows[k * HD : (k + 1) * HD, :] = columns.T
     half, quarter = n // 2, n // 4
     by_relay, relays = me == half, me == quarter
-    caches = (key_ref, value_ref)
-
-    def place(kv, slot):
-        return caches[kv].at[0, 0, pl.ds(pl.multiple_of(slot * block, block), block), :]
-
-    def block_copy(kv, t, slot):
+    def block_copy(t, slot):
         return pltpu.make_async_remote_copy(
-            sent.at[t, kv], place(kv, slot), send_sem.at[t, kv], recv_sem.at[slot, kv], device_id={"sp": t}, device_id_type=MESH
+            sent.at[t], held.at[slot], send_sem.at[t], recv_sem.at[slot], device_id={"sp": t}, device_id_type=MESH
         )
 
     def off_copy(t, slot):
@@ -96,16 +88,14 @@
             off_sent.at[t], off_held.at[slot], off_send_sem.at[t], off_recv_sem.at[slot], device_id={"sp": t}, device_id_type=MESH
         )
 
-    def to_relay(kv):
+    def to_relay():
         return pltpu.make_async_remote_copy(
-            sent.at[0, kv], relayed.at[kv], send_sem.at[0, kv], relay_recv_sem.at[kv],
-            device_id={"sp": quarter}, device_id_type=MESH,
-        )
-
-    def from_relay(kv):
+            sent.at[0], relayed, send_sem.at[0], relay_sem.at[0], device_id={"sp": quarter}, device_id_type=MESH
+        )
+
+    def from_relay():
         return pltpu.make_async_remote_copy(
-            relayed.at[kv], place(kv, half), relay_send_sem.at[kv], recv_sem.at[half, kv],
-            device_id={"sp": 0}, device_id_type=MESH,
+            relayed, held.at[half], relay_sem.at[1], recv_sem.at[half], device_id={"sp": 0}, device_id_type=MESH
         )
 
     def send(t):
@@ -113,13 +103,11 @@
 
         @pl.when(through)
         def _():
-            for kv in range(2):
-                to_relay(kv).start()
+            to_relay().start()
 
         @pl.when(jnp.logical_not(through))
         def _():
-            for kv in range(2):
-                block_copy(kv, t, me).start()
+            block_copy(t, me).start()
 
     def fold_gain(h):
         for kv in range(2):
@@ -148,24 +136,31 @@
 
             @pl.when(t == me)
             def _():
-                own = pl.ds(pl.multiple_of(me * block, block), block)
-                for kv in range(2):
-                    caches[kv][0, 0, own, :] = sent[t, kv]
+                held[me] = sent[t]
 
             @pl.when(t > me)
             def _():
                 pl.semaphore_wait(ready.at[t], 1)
                 off_copy(t, me).start()
 
-            @pl.when(t != me)
+            behind = jnp.logical_and(jnp.logical_and(me > 0, me < half), t >= me + half)
+
+            @pl.when(jnp.logical_and(t != me, jnp.logical_not(behind)))
             def _():
                 send(t)
 
+            @pl.when(jnp.logical_and(behind, t > me + half))
+            def _():
+                send(jnp.maximum(t - 1, 0))
+
+            @pl.when(jnp.logical_and(behind, t == n - 1))
+            def _():
+                send(t)
+
             @pl.when(jnp.logical_and(relays, t == n - quarter))
             def _():
-                for kv in range(2):
-                    to_relay(kv).wait_recv()
-                    from_relay(kv).start()
+                to_relay().wait_recv()
+                from_relay().start()
 
     half_block = block // 2
 
@@ -174,12 +169,17 @@
             copy.wait()
 
     wait_weights(0)
+    for h in range(1, KVH):
+        for copy in w_copies(h):
+            copy.start()
     fold_gain(0)
-    wait_weights(1)
     x_copy(0).wait()
+    for i in range(1, prompts):
+        x_copy(i).start()
     for k in range(2):
         measure_rows(0, k * half_block, half_block)
     project_heads(0, (0,))
+    wait_weights(1)
     fold_gain(1)
     hand_out(0, (0,))
 
@@ -252,14 +252,12 @@
         @pl.when(j > 0)
         def _():
             off_copy(slot, slot).wait_recv()
-            for kv in range(2):
-                block_copy(kv, slot, slot).wait_recv()
-
-        rows = pl.ds(pl.multiple_of(slot * block, block), block)
+            block_copy(slot, slot).wait_recv()
+
         off_rows = off_held[slot].astype(jnp.float32)
         off_row = jnp.concatenate([off_rows[k : k + 1] for k in range(lane_rows)], axis=1)
         off_out_ref[0, :, pl.ds(pl.multiple_of(slot * block, HD), block)] = off_row.astype(jnp.bfloat16)
-        scores = lax.dot_general(query, key_ref[0, 0, rows, :], (((1,), (1,)), ((), ())), preferred_element_type=jnp.float32)
+        scores = lax.dot_general(query, held[slot, 0], (((1,), (1,)), ((), ())), preferred_element_type=jnp.float32)
         scores = scores * (1.0 / math.sqrt(HD)) + bias + off_row
         tail = jnp.log1p(jnp.exp(-jnp.abs(scores)))
         spread = jnp.maximum(scores, 0.0) + tail
@@ -275,7 +273,7 @@
         coarse = weights.astype(jnp.bfloat16)
         fine = (weights - coarse.astype(jnp.float32)).astype(jnp.bfloat16)
         both = jnp.where(row_index < group, coarse.astype(jnp.float32), fine.astype(jnp.float32)).astype(jnp.bfloat16)
-        mixes[slot] = jnp.dot(both, value_ref[0, 0, rows, :], preferred_element_type=jnp.float32)
+        mixes[slot] = jnp.dot(both, held[slot, 1], preferred_element_type=jnp.float32)
         totals[slot] = jnp.broadcast_to(jnp.sum(spread, axis=-1, keepdims=True), (2 * group, HD))
         return carry
 
@@ -298,8 +296,7 @@
         @pl.when(j > 0)
         def _():
             off_copy(slot, slot).wait_send()
-            for kv in range(2):
-                block_copy(kv, slot, slot).wait_send()
+            block_copy(slot, slot).wait_send()
 
         return carry
 
@@ -307,17 +304,16 @@
 
     @pl.when(relays)
     def _():
-        for kv in range(2):
-            from_relay(kv).wait_send()
-
-
-def store_kernel(key_ref, value_ref, off_ref, read_ref, key_out, value_out, off_out, read_out, sems):
+        from_relay().wait_send()
+
+
+def store_kernel(held, off_ref, read_ref, key_out, value_out, off_out, read_out, sems):
     pairs = [(off_ref, off_out), (read_ref, read_out)]
-    rows = key_ref.shape[2] // STORES
+    blocks = held.shape[0] // STORES
     for k in range(STORES):
-        part = pl.ds(k * rows, rows)
-        for source, target in ((key_ref, key_out), (value_ref, value_out)):
-            pairs.append((source.at[0, 0, part, :], target.at[0, 0, part, :]))
+        part = pl.ds(k * blocks, blocks)
+        for kv, target in enumerate((key_out, value_out)):
+            pairs.append((held.at[part, kv], target.at[part]))
     copies = [pltpu.make_async_copy(source, target, sems.at[k]) for k, (source, target) in enumerate(pairs)]
     for copy in copies:
         copy.start()
@@ -333,12 +329,13 @@
     hbm = pl.BlockSpec(memory_space=pl.ANY)
     vmem = pl.BlockSpec(memory_space=pltpu.VMEM)
     smem = pl.BlockSpec(memory_space=pltpu.SMEM)
-    shapes = ((1, 1, length, HD), (1, 1, length, HD), (1, 1, length), (1, 1, group * HD))
+    small = ((1, 1, length), (1, 1, group * HD))
+    shapes = ((n, block, HD), (n, block, HD)) + small
     arrived = pl.pallas_call(
         functools.partial(kernel, n),
-        out_shape=tuple(pltpu.VMEM(shape, jnp.bfloat16) for shape in shapes),
+        out_shape=tuple(pltpu.VMEM(shape, jnp.bfloat16) for shape in ((n, 2, block, HD),) + small),
         in_specs=[hbm] * 7,
-        out_specs=(vmem, vmem, vmem, vmem),
+        out_specs=(vmem, vmem, vmem),
         scratch_shapes=[
             pltpu.VMEM((1, width), jnp.float32),
             pltpu.VMEM(stick_offsets.shape, jnp.bfloat16),
@@ -359,11 +356,10 @@
             pltpu.VMEM((n, 2 * group, HD), jnp.float32),
             pltpu.SemaphoreType.DMA((seq_count,)),
             pltpu.SemaphoreType.DMA((KVH, 2)),
-            pltpu.SemaphoreType.DMA((n, 2)),
-            pltpu.SemaphoreType.DMA((n, 2)),
             pltpu.SemaphoreType.DMA((n,)),
             pltpu.SemaphoreType.DMA((n,)),
-            pltpu.SemaphoreType.DMA((2,)),
+            pltpu.SemaphoreType.DMA((n,)),
+            pltpu.SemaphoreType.DMA((n,)),
             pltpu.SemaphoreType.DMA((2,)),
             pltpu.SemaphoreType.REGULAR((n,)),
         ],
@@ -374,14 +370,15 @@
             for array in (layer_input, input_gain.reshape(1, width), key_weight, value_weight, stick_offsets, head_bias, queries)
         )
     )
-    return pl.pallas_call(
+    keys, values, offsets, read = pl.pallas_call(
         store_kernel,
         out_shape=tuple(jax.ShapeDtypeStruct(shape, jnp.bfloat16) for shape in shapes),
-        in_specs=[vmem] * 4,
+        in_specs=[vmem] * 3,
         out_specs=(hbm,) * 4,
         scratch_shapes=[pltpu.SemaphoreType.DMA((2 * STORES + 2,))],
         compiler_params=pltpu.CompilerParams(vmem_limit_bytes=2**20),
     )(*arrived)
+    return keys.reshape(1, 1, length, HD), values.reshape(1, 1, length, HD), offsets, read
 
 
 def solution(mesh):

time: 156 us -> 156 us (level); the launches traced: 156 us -> 153 us
  Pallas kernels: 155 us -> 153 us
    pallas_call x1, Pallas kernels: 153 us -> 151 us  [shards(): pl.pallas_call(functools.partial(kernel, n), out_shape=tuple((pltpu.VMEM(...]
where the time goes in v6:
time: 156 us; the launch traced here: 153 us
  Pallas kernels  153 us (98%)
    pallas_call x1, Pallas kernels, shards(): pl.pallas_call(functools.partial(kernel, n), out_shape=tuple((pltpu.VMEM(...  151 us

profile of v6, /device:TPU:800, one launch (start us, length us, event | category | flops | bytes accessed | tf_op | source)
XLA Modules:
  0.0 153.2 jit_solution(835395949527389320)
XLA Ops:
  0.6 150.8 %shard_map.102 = (bf16[16,2,384,128]{3,2,1,0:T(8,128)(2,1)S(1)}, bf16[1,1,6144]{2,1,0:T(2,128)(2,1)S(1)}, bf16[1,1,512]{2,1,0:T(2,128)(2,1)S(1)}) custom-call(bf16[4,384,2048]{2,1,0:T(8,128)(2,1)} %x_ref.1, f32[1,2048]{1,0:T(1,128)} %bitcast.3, bf16[2048,512]{1,0:T(8,128)(2,1)} %wk_ref.1, bf16[2048,512]{1,0:T(8,128)(2,1)} %wv_ref.1, ...), custom_call_target="tpu_custom_call" | custom-call | tf_op jit(solution)/shard_map/pallas_call | solution.py:334
  151.5 1.8 %shard_map.103 = (bf16[16,384,128]{2,1,0:T(8,128)(2,1)}, bf16[16,384,128]{2,1,0:T(8,128)(2,1)}, bf16[1,1,6144]{2,1,0:T(2,128)(2,1)}, bf16[1,1,512]{2,1,0:T(2,128)(2,1)}) custom-call(bf16[16,2,384,128]{3,2,1,0:T(8,128)(2,1)S(1)} %get-tuple-element.11.held, bf16[1,1,6144]{2,1,0:T(2,128)(2,1)S(1)} %get-tuple-element.12.off_ref, ...), custom_call_target="tpu_custom_call" | custom-call | tf_op jit(solution)/shard_map/pallas_call | solution.py:373
